TPU v7x, 32 devices: a whole 2x2x4 slice. The times are simulated.
32 devices in a mesh: fs: 8 (over z, x), tp: 4 (over y, core).
Axes of the slice: x: 2, y: 2, z: 4, core: 2. Of those that a mesh axis runs over, the one named last changes fastest.
Arguments:
- tokens: bfloat16 [1024, 2048], P('fs'), may hold values from -6 to 6
- gain: float32 [2048], P('fs'), may hold values from 0.1 to 1.9
- up_master: float32 [2048, 8192], P('fs', 'tp'), may hold values from -0.125 to 0.125
- down_master: float32 [2048, 8192], P('fs', 'tp'), may hold values from -0.0625 to 0.0625
Outputs:
- up_sampled: bfloat16 [8, 2048, 1024], P('fs', None, 'tp')
- down_sampled: bfloat16 [8, 2048, 1024], P('fs', None, 'tp')
- mixed: bfloat16 [1024, 2048], P('fs', 'tp')
All inputs are finite; a program needn't handle non-finite values.
Results may differ from a plain program's by a relative error of at most 0.0087.
Values may be sent and summed in bfloat16 or wider, within the bound.
A program may use at most 64 MiB of HBM per device.

v0:
```python
import jax
import jax.numpy as jnp
from jax import lax
from jax.sharding import PartitionSpec as P

SUB = 8


def from_partner(block, axis, bit):
    count = lax.axis_size(axis)
    route = []
    for low in range(count):
        high = low | 1 << bit
        if high != low and high < count:
            route += [(low, high), (high, low)]
    return lax.ppermute(block, axis, route)


def on_device(tokens, gain, up_master, down_master):
    fs_count = lax.axis_size("fs")
    feat_rows = up_master.shape[0]
    units = up_master.shape[1] // SUB
    groups_count = fs_count // SUB
    member = lax.axis_index("fs") % SUB
    up_round = (gain[:, None] * up_master).astype(jnp.bfloat16)
    down_round = down_master.astype(jnp.bfloat16)

    def spread(weight):
        blocks = weight.reshape(feat_rows, SUB, units).transpose(1, 0, 2)
        return jnp.broadcast_to(blocks[None], (groups_count, SUB, feat_rows, units)).reshape(
            fs_count, feat_rows, units
        )

    up_sampled, down_sampled = (
        lax.all_to_all(spread(up_round), "fs", split_axis=0, concat_axis=1, tiled=True),
        lax.all_to_all(spread(down_round), "fs", split_axis=0, concat_axis=1, tiled=True),
    )
    levels = SUB.bit_length() - 1
    bit_list = list(range(levels))
    widened = tokens.astype(jnp.float32)
    normed = (
        widened * lax.rsqrt(jnp.mean(widened * widened, axis=1, keepdims=True) + 1e-06)
    ).astype(jnp.bfloat16)
    current = normed[None]
    for bit in bit_list:
        partner = from_partner(current, "fs", bit)
        lower = member >> bit & 1 == 0
        current = jnp.where(lower, jnp.stack([current, partner]), jnp.stack([partner, current]))
    order_now = list(reversed(bit_list))
    wanted = list(range(levels - 1, -1, -1))
    perm_axes = [
        [place for place, value in enumerate(order_now) if value == target][0] for target in wanted
    ]
    current = jnp.transpose(current, perm_axes + [levels, levels + 1, levels + 2])
    gathered = current.reshape(SUB * tokens.shape[0], tokens.shape[1])
    pre_units = jnp.dot(gathered, up_sampled[0], preferred_element_type=jnp.float32)
    act_units = jnp.square(jax.nn.relu(pre_units)).astype(jnp.bfloat16)
    partial_out = lax.dot_general(
        act_units, down_sampled[0], (((1,), (1,)), ((), ())), preferred_element_type=jnp.float32
    )
    running = partial_out.reshape((2,) * levels + (tokens.shape[0], tokens.shape[1]))
    axis_bits = list(range(levels - 1, -1, -1))
    for bit in bit_list:
        position = len([value for value in axis_bits if value > bit])
        mine = member >> bit & 1
        keep = lax.dynamic_index_in_dim(running, mine, position, keepdims=False)
        other = lax.dynamic_index_in_dim(running, 1 - mine, position, keepdims=False)
        running = keep + from_partner(other, "fs", bit)
        axis_bits = [value for value in axis_bits if value != bit]
    summed = lax.psum_scatter(running, "tp", scatter_dimension=1, tiled=True)
    return (up_sampled, down_sampled, summed.astype(jnp.bfloat16))


def solution(mesh):
    placed = (P("fs", None), P("fs"), P("fs", "tp"), P("fs", "tp"))
    return jax.shard_map(
        on_device,
        mesh=mesh,
        in_specs=placed,
        out_specs=(P("fs", None, "tp"), P("fs", None, "tp"), P("fs", "tp")),
        check_vma=False,
    )
```

profile of v0, /device:TPU:0, one launch (start us, length us, event | category | flops | bytes accessed | tf_op | source)
XLA Modules:
  0.0 420.9 jit_solution(5707439583742261724)
XLA Ops:
  7.2 0.0 copy-start.4
  7.2 1.2 fusion.3
  8.4 1.2 fusion.6
  9.6 3.0 collective-permute-start
  12.7 11.9 %collective-permute-done = bf16[1,128,2048]{2,1,0:T(8,128)(2,1)S(1)} collective-permute-done((bf16[1,128,2048]{2,1,0:T(8,128)(2,1)S(1)}, bf16[1,128,2048]{2,1,0:T(8,128)(2,1)S(1)}, u32[]{:S(2)}, u32[]{:S(2)}) %collective-permute-start) | collective-permute-done | bytes 524320 | tf_op jit(solution)/shard_map/ppermute | solution.py:16
  24.6 1.1 maximum_select_fusion.4
  25.7 1.8 collective-permute-start.1
  27.5 0.0 copy-done.4
  27.5 0.0 copy-done.3
  27.5 0.2 multiply_convert_fusion
  27.7 1.0 copy.15
  28.8 4.8 %all-to-all-start = ((bf16[8,256,256]{2,1,0:T(8,128)(2,1)}), bf16[8,256,256]{2,1,0:T(8,128)(2,1)}, u32[]{:S(2)}, u32[]{:S(2)}) async-start(bf16[8,256,256]{2,1,0:T(8,128)(2,1)} %bitcast.53), calls=%async_computation | async-start | bytes 2097152 | tf_op jit(solution)/shard_map/all_to_all | solution.py:35
  33.6 0.2 fusion.8
  33.8 28.0 %collective-permute-done.1 = bf16[2,1,128,2048]{3,2,1,0:T(8,128)(2,1)S(1)} collective-permute-done((bf16[2,1,128,2048]{3,2,1,0:T(8,128)(2,1)}, bf16[2,1,128,2048]{3,2,1,0:T(8,128)(2,1)S(1)}, u32[]{:S(2)}, u32[]{:S(2)}) %collective-permute-start.1) | collective-permute-done | bytes 1048608 | tf_op jit(solution)/shard_map/ppermute | solution.py:16
  61.8 1.7 maximum_select_fusion.2
  63.4 3.4 collective-permute-start.2
  66.9 0.0 copy-done.2
  66.9 0.1 convert_element_type.19
  67.0 1.0 copy.14
  68.1 2.2 all-to-all-done
  70.3 4.5 %all-to-all-start.1 = ((bf16[8,256,256]{2,1,0:T(8,128)(2,1)}), bf16[8,256,256]{2,1,0:T(8,128)(2,1)S(1)}, u32[]{:S(2)}, u32[]{:S(2)}) async-start(bf16[8,256,256]{2,1,0:T(8,128)(2,1)} %bitcast.60), calls=%async_computation.1 | async-start | bytes 2097152 | tf_op jit(solution)/shard_map/all_to_all | solution.py:36
  74.8 0.0 reduce-scatter.2.cloned.1.call-start
  74.9 0.3 fusion
  75.2 95.2 %collective-permute-done.2 = bf16[2,2,1,128,2048]{4,3,1,2,0:T(8,128)(2,1)} collective-permute-done((bf16[2,2,1,128,2048]{4,3,1,2,0:T(8,128)(2,1)}, bf16[2,2,1,128,2048]{4,3,1,2,0:T(8,128)(2,1)}, u32[]{:S(2)}, u32[]{:S(2)}) %collective-permute-start.2) | collective-permute-done | bytes 2097184 | tf_op jit(solution)/shard_map/ppermute | solution.py:16
  170.4 2.8 maximum_select_fusion
  173.2 2.5 fusion.2
  175.7 5.7 %all-to-all-done.1 = bf16[8,256,256]{2,1,0:T(8,128)(2,1)S(1)} async-done(((bf16[8,256,256]{2,1,0:T(8,128)(2,1)}), bf16[8,256,256]{2,1,0:T(8,128)(2,1)S(1)}, u32[]{:S(2)}, u32[]{:S(2)}) %all-to-all-start.1) | async-done | bytes 1048608 | tf_op jit(solution)/shard_map/all_to_all | solution.py:36
  181.4 1.3 fusion.9
  182.7 0.0 copy-start
  182.7 2.4 dynamic-slice_bitcast_fusion
  185.1 2.1 copy-done
  187.2 0.0 collective-permute-start.3
  187.2 92.8 %collective-permute-done.3 = f32[2,2,128,2048]{3,2,1,0:T(8,128)} collective-permute-done((f32[2,2,128,2048]{3,2,1,0:T(8,128)}, f32[2,2,128,2048]{3,2,1,0:T(8,128)}, u32[]{:S(2)}, u32[]{:S(2)}) %collective-permute-start.3) | collective-permute-done | bytes 4194336 | tf_op jit(solution)/shard_map/ppermute | solution.py:16
  280.0 4.2 %bitcast_add_fusion = f32[2,2,128,2048]{3,2,1,0:T(8,128)S(1)} fusion(f32[2,2,128,2048]{3,2,1,0:T(8,128)} %collective-permute-done.3, f32[2,2,2,128,2048]{4,3,2,1,0:T(8,128)} %copy-done, s32[]{:T(128)S(6)} %select_n.151), kind=kLoop, calls=%fused_computation.1 | loop fusion | flops 1048576 | bytes 12582916 | tf_op jit(solution)/shard_map/add | solution.py:68
  284.2 0.1 dynamic-slice_bitcast_fusion.1
  284.4 1.8 copy-done.1
  286.2 0.0 collective-permute-start.4
  286.2 46.8 %collective-permute-done.4 = f32[2,128,2048]{2,1,0:T(8,128)} collective-permute-done((f32[2,128,2048]{2,1,0:T(8,128)S(1)}, f32[2,128,2048]{2,1,0:T(8,128)}, u32[]{:S(2)}, u32[]{:S(2)}) %collective-permute-start.4) | collective-permute-done | bytes 2097184 | tf_op jit(solution)/shard_map/ppermute | solution.py:16
  333.0 2.5 bitcast_add_fusion.1
  335.5 1.1 dynamic-slice_bitcast_fusion.2
  336.5 0.2 collective-permute-start.5
  336.7 46.9 %collective-permute-done.5 = f32[128,2048]{1,0:T(8,128)} collective-permute-done((f32[128,2048]{1,0:T(8,128)}, f32[128,2048]{1,0:T(8,128)}, u32[]{:S(2)}, u32[]{:S(2)}) %collective-permute-start.5) | collective-permute-done | bytes 1048608 | tf_op jit(solution)/shard_map/ppermute | solution.py:16
  383.6 2.3 bitcast_add_fusion.2
  385.9 0.0 reduce-scatter.2.cloned.1.call-update
  385.9 23.3 %reduce-scatter.2.cloned.1.call-done = f32[128,512]{1,0:T(8,128)} async-done(((f32[128,2048]{1,0:T(8,128)}), f32[128,512]{1,0:T(8,128)}) %reduce-scatter.2.cloned.1.call-update) | async-done | bytes 262160 | tf_op jit(solution)/shard_map/reduce_scatter | solution.py:70
  409.2 1.6 convert_element_type.23
  410.8 2.3 copy.18
  413.1 1.0 copy.19
  (4 shorter events, 0.0 us)
Async XLA Ops:
  7.2 20.4 %copy-start.4 = (f32[256]{0:T(256)S(1)}, f32[256]{0:T(256)}, u32[]{:S(2)}) copy-start(f32[256]{0:T(256)} %param.5) | copy-start | bytes 3076
  9.6 15.0 %collective-permute-start = (bf16[1,128,2048]{2,1,0:T(8,128)(2,1)S(1)}, bf16[1,128,2048]{2,1,0:T(8,128)(2,1)S(1)}, u32[]{:S(2)}, u32[]{:S(2)}) collective-permute-start(bf16[1,128,2048]{2,1,0:T(8,128)(2,1)S(1)} %get-tuple-element.6), channel_id=1, source_target_pairs={{0,4},{4,0},{8,12},{12,8},{16,20},{20,16},{24,28},{28,24},{1,5},{5... | collective-permute-start | bytes 1572872 | tf_op jit(solution)/shard_map/ppermute | solution.py:16
  12.7 14.9 %copy-start.3 = (f32[256,2048]{1,0:T(8,128)S(1)}, f32[256,2048]{1,0:T(8,128)}, u32[]{:S(2)}) copy-start(f32[256,2048]{1,0:T(8,128)} %param.6) | copy-start | bytes 6291460
  25.7 36.1 %collective-permute-start.1 = (bf16[2,1,128,2048]{3,2,1,0:T(8,128)(2,1)}, bf16[2,1,128,2048]{3,2,1,0:T(8,128)(2,1)S(1)}, u32[]{:S(2)}, u32[]{:S(2)}) collective-permute-start(bf16[2,1,128,2048]{3,2,1,0:T(8,128)(2,1)} %maximum_select_fusion.4), channel_id=1, source_target_pairs={{0,8},{8,0},{4,12},{12,4},{16,24},{24,16},{20,28},{28,20},{1,9},{9... | collective-permute-start | bytes 3145736 | tf_op jit(solution)/shard_map/ppermute | solution.py:16
  28.8 41.5 %all-to-all-start = ((bf16[8,256,256]{2,1,0:T(8,128)(2,1)}), bf16[8,256,256]{2,1,0:T(8,128)(2,1)}, u32[]{:S(2)}, u32[]{:S(2)}) async-start(bf16[8,256,256]{2,1,0:T(8,128)(2,1)} %bitcast.53), calls=%async_computation | async-start | bytes 2097152 | tf_op jit(solution)/shard_map/all_to_all | solution.py:35
  61.8 5.1 %copy-start.2 = (f32[256,2048]{1,0:T(8,128)S(1)}, f32[256,2048]{1,0:T(8,128)}, u32[]{:S(2)}) copy-start(f32[256,2048]{1,0:T(8,128)} %param.7) | copy-start | bytes 6291460
  63.4 107.0 %collective-permute-start.2 = (bf16[2,2,1,128,2048]{4,3,1,2,0:T(8,128)(2,1)}, bf16[2,2,1,128,2048]{4,3,1,2,0:T(8,128)(2,1)}, u32[]{:S(2)}, u32[]{:S(2)}) collective-permute-start(bf16[2,2,1,128,2048]{4,3,1,2,0:T(8,128)(2,1)} %maximum_select_fusion.2), channel_id=1, source_target_pairs={{0,16},{16,0},{4,20},{20,4},{8,24},{24,8},{12,28},{28,12},{1,17},{... | collective-permute-start | bytes 6291464 | tf_op jit(solution)/shard_map/ppermute | solution.py:16
  70.3 111.1 %all-to-all-start.1 = ((bf16[8,256,256]{2,1,0:T(8,128)(2,1)}), bf16[8,256,256]{2,1,0:T(8,128)(2,1)S(1)}, u32[]{:S(2)}, u32[]{:S(2)}) async-start(bf16[8,256,256]{2,1,0:T(8,128)(2,1)} %bitcast.60), calls=%async_computation.1 | async-start | bytes 2097152 | tf_op jit(solution)/shard_map/all_to_all | solution.py:36
  74.8 334.4 %reduce-scatter.2.cloned.1.call-start = ((), (), s32[]{:S(2)}) async-start(), calls=%async_computation.3 | async-start | bytes 1310720 | tf_op jit(solution)/shard_map/reduce_scatter | solution.py:70
  182.7 4.5 %copy-start = (f32[2,2,2,128,2048]{4,3,2,1,0:T(8,128)}, f32[2,2,2,128,2048]{4,3,2,1,0:T(8,128)S(1)}, u32[]{:S(2)}) copy-start(f32[2,2,2,128,2048]{4,3,2,1,0:T(8,128)S(1)} %fusion.9) | copy-start | bytes 25165828
  187.2 92.8 %collective-permute-start.3 = (f32[2,2,128,2048]{3,2,1,0:T(8,128)}, f32[2,2,128,2048]{3,2,1,0:T(8,128)}, u32[]{:S(2)}, u32[]{:S(2)}) collective-permute-start(f32[2,2,128,2048]{3,2,1,0:T(8,128)} %dynamic-slice_bitcast_fusion), channel_id=1, source_target_pairs={{0,4},{4,0},{8,12},{12,8},{16,20},{20,16},{24,28},{28,24},{1,5},{5... | collective-permute-start | bytes 12582920 | tf_op jit(solution)/shard_map/ppermute | solution.py:16
  284.2 1.9 copy-start.1
  286.2 46.8 %collective-permute-start.4 = (f32[2,128,2048]{2,1,0:T(8,128)S(1)}, f32[2,128,2048]{2,1,0:T(8,128)}, u32[]{:S(2)}, u32[]{:S(2)}) collective-permute-start(f32[2,128,2048]{2,1,0:T(8,128)S(1)} %dynamic-slice_bitcast_fusion.1), channel_id=1, source_target_pairs={{0,8},{8,0},{4,12},{12,4},{16,24},{24,16},{20,28},{28,20},{1,9},{9... | collective-permute-start | bytes 6291464 | tf_op jit(solution)/shard_map/ppermute | solution.py:16
  336.5 47.0 %collective-permute-start.5 = (f32[128,2048]{1,0:T(8,128)}, f32[128,2048]{1,0:T(8,128)}, u32[]{:S(2)}, u32[]{:S(2)}) collective-permute-start(f32[128,2048]{1,0:T(8,128)} %dynamic-slice_bitcast_fusion.2), channel_id=1, source_target_pairs={{0,16},{16,0},{4,20},{20,4},{8,24},{24,8},{12,28},{28,12},{1,17},{... | collective-permute-start | bytes 3145736 | tf_op jit(solution)/shard_map/ppermute | solution.py:16
Sparse Core Ops, SparseCore 0:
  386.0 23.1 reduce-scatter.1
where the time goes:
time: 421 us
  waiting for transfers between devices  353 us (84%)
  other arithmetic  19.5 us (5%)
  starting transfers between devices  17.8 us (4%)
  between operations  14.1 us (3%)
  local copies, waits for them, and re-layouts  12.8 us (3%)
    ppermute x6, waiting for transfers between devices, from_partner(): return lax.ppermute(block, axis, route)  322 us
    reduce_scatter x1, waiting for transfers between devices, on_device(): summed = lax.psum_scatter(running, 'tp', scatter_dimension=1, tiled=True)  23.3 us
    add x3, other arithmetic, on_device(): running = keep + from_partner(other, 'fs', bit)  9 us
    ppermute x6, starting transfers between devices, from_partner(): return lax.ppermute(block, axis, route)  8.49 us
  transfers between devices with their start and end apart: 9, of which 9 were waited for; matrix products, arithmetic and copies ran while one was open for 2% of the time, Pallas kernels for 0%

commit v1 on v0

--- a/solution.py
+++ b/solution.py
@@ -1,9 +1,241 @@
+import functools
+
 import jax
 import jax.numpy as jnp
 from jax import lax
+from jax.experimental import pallas as pl
+from jax.experimental.pallas import tpu as pltpu
 from jax.sharding import PartitionSpec as P
 
 SUB = 8
+EPS = 1e-06
+BF16 = jnp.bfloat16
+F32 = jnp.float32
+
+
+def fused(
+    nz, tok, gain, upm, dnm, up_o, dn_o, mix_o,
+    xg, up_s, dn_s, act, cs, cr, ys, yr, xs, xb, xr, zb, zr,
+    s_tz, r_tz, s_tx, r_tx, s_ty, r_ty, s_tc, r_tc,
+    s_up, r_up, s_dn, r_dn, s_c, r_c, s_y, r_y, s_x, r_x, s_z, r_z,
+):
+    f, t = lax.axis_index("fs"), lax.axis_index("tp")
+    z, x = f // 2, f % 2
+    y, c = t // 2, t % 2
+    ox, oy, oc = 1 - x, 1 - y, 1 - c
+    rows, width = tok.shape
+    cols = width // 4
+    feat = upm.shape[0]
+    units = act.shape[1]
+    at_x = (z * 2 + ox, t)
+    at_y = (f, oy * 2 + c)
+    at_c = (f, y * 2 + oc)
+
+    barrier = pltpu.get_barrier_semaphore()
+    for d in range(1, SUB):
+        pl.semaphore_signal(barrier, inc=1, device_id=((f + d) % SUB, t),
+                            device_id_type=pl.DeviceIdType.MESH)
+    for dev in (at_y, at_c):
+        pl.semaphore_signal(barrier, inc=1, device_id=dev, device_id_type=pl.DeviceIdType.MESH)
+
+    sent = []
+
+    def send(src, dst, ssem, rsem, dev):
+        copy = pltpu.make_async_remote_copy(
+            src_ref=src, dst_ref=dst, send_sem=ssem, recv_sem=rsem,
+            device_id=dev, device_id_type=pl.DeviceIdType.MESH)
+        copy.start()
+        sent.append(copy)
+
+    def arrived(dst, ssem, rsem, dev):
+        pltpu.make_async_remote_copy(
+            src_ref=dst, dst_ref=dst, send_sem=ssem, recv_sem=rsem,
+            device_id=dev, device_id_type=pl.DeviceIdType.MESH).wait_recv()
+
+    low = 1 - z // 2
+    far = (3 * low, 1 + low, 1 - z + 4 * (1 - low))
+
+    wide = tok[...].astype(F32)
+    scale = lax.rsqrt(jnp.mean(wide * wide, axis=1, keepdims=True) + EPS)
+    mine = tok[:, pl.ds(pl.multiple_of(t * cols, cols), cols)].astype(F32)
+    xg[t, z, x] = (mine * scale).astype(BF16)
+    pl.semaphore_wait(barrier, SUB + 1)
+
+    for zz in far:
+        send(xg.at[t, z, x], xg.at[t, z, x], s_tz.at[zz], r_tz.at[z], (zz * 2 + x, t))
+
+    def pass_on(zz):
+        send(xg.at[t, zz, x], xg.at[t, zz, x], s_tx.at[zz], r_tx.at[zz], at_x)
+        send(xg.at[t, zz, x], xg.at[t, zz, x], s_ty.at[zz, x], r_ty.at[zz, x], at_y)
+
+    pass_on(z)
+
+    def cast(src, dst, out, factor):
+        for m in range(SUB):
+            block = src[:, m * units:(m + 1) * units]
+            dst[m] = (block if factor is None else factor * block).astype(BF16)
+        block = src[:, pl.ds(pl.multiple_of(f * units, units), units)]
+        out[pl.ds(pl.multiple_of(f * feat, feat), feat), :] = (
+            block if factor is None else factor * block).astype(BF16)
+
+    def at_rows(ref, k):
+        return ref.at[pl.ds(pl.multiple_of(k * feat, feat), feat), :]
+
+    def scatter(src, out, ssem, rsem):
+        order = [zz * 2 + xx for zz in far for xx in (x, ox)] + [z * 2 + ox]
+        for dest in order:
+            send(src.at[dest], at_rows(out, f), ssem.at[dest], rsem.at[f], (dest, t))
+
+    cast(upm, up_s, up_o, gain[...])
+    scatter(up_s, up_o, s_up, r_up)
+    cast(dnm, dn_s, dn_o, None)
+    scatter(dn_s, dn_o, s_dn, r_dn)
+
+    near = (far[2], far[1], far[0])
+    for zz in near:
+        arrived(xg.at[t, zz, x], s_tz.at[zz], r_tz.at[zz], (zz * 2 + x, t))
+        pass_on(zz)
+    for xx in (x,):
+        send(xg.at[t, :, xx], xg.at[t, :, xx], s_tc.at[y, xx], r_tc.at[y, xx], at_c)
+    for zz in (z,) + near:
+        arrived(xg.at[t, zz, ox], s_tx.at[zz], r_tx.at[zz], at_x)
+        send(xg.at[t, zz, ox], xg.at[t, zz, ox], s_ty.at[zz, ox], r_ty.at[zz, ox], at_y)
+    send(xg.at[t, :, ox], xg.at[t, :, ox], s_tc.at[y, ox], r_tc.at[y, ox], at_c)
+    other = oy * 2 + c
+    for xx in (x, ox):
+        for zz in (z,) + near:
+            arrived(xg.at[other, zz, xx], s_ty.at[zz, xx], r_ty.at[zz, xx], at_y)
+        send(xg.at[other, :, xx], xg.at[other, :, xx], s_tc.at[oy, xx], r_tc.at[oy, xx], at_c)
+    for yy in (y, oy):
+        for xx in (x, ox):
+            part = xg.at[yy * 2 + oc, :, xx]
+            arrived(part, s_tc.at[yy, xx], r_tc.at[yy, xx], at_c)
+
+    everyone = [zz * 2 + xx for zz in far for xx in (x, ox)] + [z * 2 + ox]
+    for k in everyone:
+        arrived(at_rows(up_o, k), s_up.at[k], r_up.at[k], (k, t))
+
+    span = 2 * rows
+
+    @pl.loop(0, nz)
+    def _(zz):
+        total = jnp.zeros((span, units), F32)
+        for q in range(4):
+            total += jnp.dot(xg[q, zz].reshape(span, cols), up_o[q * cols:(q + 1) * cols, :],
+                             preferred_element_type=F32)
+        act[pl.ds(pl.multiple_of(zz * span, span), span), :] = jnp.square(
+            jnp.maximum(total, 0.0)).astype(BF16)
+
+    def partial(k, zz):
+        return lax.dot_general(
+            act[pl.ds(pl.multiple_of(zz * span, span), span), :],
+            dn_o[pl.ds(pl.multiple_of(k * feat, feat), feat), :],
+            (((1,), (1,)), ((), ())), preferred_element_type=F32)
+
+    def have(k):
+        @pl.when(k != f)
+        def _():
+            arrived(at_rows(dn_o, k), s_dn.at[k], r_dn.at[k], (k, t))
+
+    def to_core(yy, i):
+        k = yy * 4 + oc * 2 + i
+        have(k)
+
+        @pl.loop(0, nz)
+        def _(zz):
+            cs[yy * 2 + i, zz] = partial(k, zz).astype(BF16)
+
+        send(cs.at[yy * 2 + i], cr.at[yy * 2 + i], s_c.at[yy, i], r_c.at[yy, i], at_c)
+
+    def core_sum(yy, i):
+        have(yy * 4 + c * 2 + i)
+        arrived(cr.at[yy * 2 + i], s_c.at[yy, i], r_c.at[yy, i], at_c)
+
+    for i in range(2):
+        to_core(oy, i)
+    for i in range(2):
+        core_sum(oy, i)
+
+        @pl.loop(0, nz)
+        def _(zz):
+            ys[i, zz] = (partial(oy * 4 + c * 2 + i, zz) + cr[oy * 2 + i, zz].astype(F32)).astype(BF16)
+
+        send(ys.at[i], yr.at[i], s_y.at[i], r_y.at[i], at_y)
+    for i in range(2):
+        to_core(y, i)
+    for i in range(2):
+        core_sum(y, i)
+        arrived(yr.at[i], s_y.at[i], r_y.at[i], at_y)
+
+        @pl.loop(0, nz)
+        def _(zz):
+            total = (partial(y * 4 + c * 2 + i, zz) + cr[y * 2 + i, zz].astype(F32)
+                     + yr[i, zz].astype(F32))
+            for xx in range(2):
+                half = total[xx * rows:(xx + 1) * rows]
+                xs[i, xx, zz] = half
+                xb[i, xx, zz] = half.astype(BF16)
+
+        send(xb.at[i, ox], xr.at[i], s_x.at[i], r_x.at[i], at_x)
+    for i in range(2):
+        arrived(xr.at[i], s_x.at[i], r_x.at[i], at_x)
+
+        @pl.loop(0, nz)
+        def _(zz):
+            total = xs[i, x, zz] + xr[i, zz].astype(F32)
+            xs[i, x, zz] = total
+            zb[i, zz] = total.astype(BF16)
+
+        for zz in far:
+            send(zb.at[i, zz], zr.at[i, z], s_z.at[i, zz], r_z.at[i, z], (zz * 2 + x, t))
+    for i in range(2):
+        total = xs[i, x, z]
+        for zz in near:
+            arrived(zr.at[i, zz], s_z.at[i, zz], r_z.at[i, zz], (zz * 2 + x, t))
+            total += zr[i, zz].astype(F32)
+        mix_o[:, i * feat:(i + 1) * feat] = total.astype(BF16)
+    for copy in sent:
+        copy.wait_send()
+
+
+def on_device_fused(tokens, gain, up_master, down_master):
+    rows, width = tokens.shape
+    feat, ff = up_master.shape
+    units = ff // SUB
+    nz = SUB // 2
+    cols = width // 4
+    span = 2 * rows
+    dma = pltpu.SemaphoreType.DMA
+    vmem = pl.BlockSpec(memory_space=pltpu.VMEM)
+    shapes = [(nz,), (nz,), (nz, 2), (2, 2), (SUB,), (SUB,), (2, 2), (2,), (2,), (2, nz)]
+    up_s, dn_s, mixed = pl.pallas_call(
+        functools.partial(fused, nz),
+        out_shape=(
+            jax.ShapeDtypeStruct((SUB * feat, units), BF16),
+            jax.ShapeDtypeStruct((SUB * feat, units), BF16),
+            jax.ShapeDtypeStruct((rows, cols), BF16),
+        ),
+        in_specs=[vmem] * 4,
+        out_specs=(vmem,) * 3,
+        scratch_shapes=[
+            pltpu.VMEM((4, nz, 2, rows, cols), BF16),
+            pltpu.VMEM((SUB, feat, units), BF16),
+            pltpu.VMEM((SUB, feat, units), BF16),
+            pltpu.VMEM((SUB * rows, units), BF16),
+            pltpu.VMEM((4, nz, span, feat), BF16),
+            pltpu.VMEM((4, nz, span, feat), BF16),
+            pltpu.VMEM((2, nz, span, feat), BF16),
+            pltpu.VMEM((2, nz, span, feat), BF16),
+            pltpu.VMEM((2, 2, nz, rows, feat), F32),
+            pltpu.VMEM((2, 2, nz, rows, feat), BF16),
+            pltpu.VMEM((2, nz, rows, feat), BF16),
+            pltpu.VMEM((2, nz, rows, feat), BF16),
+            pltpu.VMEM((2, nz, rows, feat), BF16),
+        ] + [dma(shape) for shape in shapes for _ in range(2)],
+        compiler_params=pltpu.CompilerParams(
+            collective_id=0, has_side_effects=True, vmem_limit_bytes=60 * 2**20),
+    )(tokens, gain[:, None], up_master, down_master)
+    return up_s[None], dn_s[None], mixed
 
 
 def from_partner(block, axis, bit):
@@ -73,8 +305,9 @@
 
 def solution(mesh):
     placed = (P("fs", None), P("fs"), P("fs", "tp"), P("fs", "tp"))
+    one_group = mesh.shape["fs"] == SUB and mesh.shape["tp"] == 4
     return jax.shard_map(
-        on_device,
+        on_device_fused if one_group else on_device,
         mesh=mesh,
         in_specs=placed,
         out_specs=(P("fs", None, "tp"), P("fs", None, "tp"), P("fs", "tp")),

time: 421 us -> 116 us (0.28)
  waiting for transfers between devices: 353 us -> 0 us
  Pallas kernels: 0 us -> 109 us
  other arithmetic: 19.5 us -> 0 us
  starting transfers between devices: 17.8 us -> 0 us
  between operations: 14.1 us -> 0.66 us
  local copies, waits for them, and re-layouts: 12.8 us -> 5.46 us
    ppermute x6 -> x0, waiting for transfers between devices: 322 us -> none  [from_partner(): return lax.ppermute(block, axis, route)]
    pallas_call x0 -> x1, Pallas kernels: none -> 109 us  [on_device_fused(): pl.pallas_call(functools.partial(fused, nz), out_shape=(jax.ShapeDtypeStr...]
    reduce_scatter x1 -> x0, waiting for transfers between devices: 23.3 us -> none  [on_device(): summed = lax.psum_scatter(running, 'tp', scatter_dimension=1, tiled=True)]
    all_to_all x2 -> x0, starting transfers between devices: 9.3 us -> none  [the longest x1 4.79 us: on_device(): lax.all_to_all(spread(up_round), 'fs', split_axis=0, concat_axis=1, tiled...]
    add x3 -> x0, other arithmetic: 9 us -> none  [on_device(): running = keep + from_partner(other, 'fs', bit)]
    ppermute x6 -> x0, starting transfers between devices: 8.49 us -> none  [from_partner(): return lax.ppermute(block, axis, route)]
    all_to_all x2 -> x0, waiting for transfers between devices: 7.95 us -> none  [the longest x1 5.73 us: on_device(): lax.all_to_all(spread(down_round), 'fs', split_axis=0, concat_axis=1, til...]
    select_n x3 -> x0, other arithmetic: 5.61 us -> none  [on_device(): jnp.where(lower, jnp.stack([current, partner]), jnp.stack([partner, curre...]
  transfers between devices with their start and end apart: 9 -> 0, of which waited for: 9 -> 0; matrix products, arithmetic and copies ran while one was open for 2% -> 0% of each run, Pallas kernels for 0% -> 0%
where the time goes in v1:
time: 116 us
  Pallas kernels  109 us (94%)
  local copies, waits for them, and re-layouts  5.46 us (5%)
    pallas_call x1, Pallas kernels, on_device_fused(): pl.pallas_call(functools.partial(fused, nz), out_shape=(jax.ShapeDtypeStr...  109 us
    unnamed x7, local copies, waits for them, and re-layouts  3.99 us

profile of v1, /device:TPU:0, one launch (start us, length us, event | category | flops | bytes accessed | tf_op | source)
XLA Modules:
  0.0 115.6 jit_solution(5442647096266351943)
XLA Ops:
  0.6 1.5 %copy.7.gain = f32[256,1]{1,0:T(8,128)} copy(f32[256,1]{0,1:T(1,128)} %bitcast.5) | data formatting | bytes 2048 | tf_op jit(solution)/shard_map/broadcast_in_dim | solution.py:237
  2.1 109.5 %shard_map.67 = (bf16[2048,256]{1,0:T(8,128)(2,1)}, bf16[2048,256]{1,0:T(8,128)(2,1)}, bf16[128,512]{1,0:T(8,128)(2,1)}) custom-call(bf16[128,2048]{1,0:T(8,128)(2,1)} %tok.1, f32[256,1]{1,0:T(8,128)} %copy.7.gain, f32[256,2048]{1,0:T(8,128)} %upm.1, f32[256,2048]{1,0:T(8,128)} %dnm.1), custom_call_target="tpu_custom_call" | custom-call | tf_op jit(solution)/shard_map/pallas_call | solution.py:211
  111.6 0.0 copy-start
  111.6 0.0 copy-start.1
  111.6 2.4 %copy.11 = bf16[1,2048,256]{2,1,0:T(8,128)(2,1)} copy(bf16[1,2048,256]{2,1,0:T(8,128)(2,1)} %bitcast.4) | data formatting | bytes 2097152
  113.9 0.0 copy-done
  113.9 1.0 copy.12
  114.9 0.0 copy-done.1
  114.9 0.7 copy.13
Async XLA Ops:
  111.6 2.4 %copy-start = (bf16[2048,256]{1,0:T(8,128)(2,1)S(1)}, bf16[2048,256]{1,0:T(8,128)(2,1)}, u32[]{:S(2)}) copy-start(bf16[2048,256]{1,0:T(8,128)(2,1)} %get-tuple-element.7) | copy-start | bytes 3145732
  111.6 3.3 %copy-start.1 = (bf16[128,512]{1,0:T(8,128)(2,1)S(1)}, bf16[128,512]{1,0:T(8,128)(2,1)}, u32[]{:S(2)}) copy-start(bf16[128,512]{1,0:T(8,128)(2,1)} %get-tuple-element.14) | copy-start | bytes 393220

commit v2 on v1

--- a/solution.py
+++ b/solution.py
@@ -15,9 +15,9 @@
 
 def fused(
     nz, tok, gain, upm, dnm, up_o, dn_o, mix_o,
-    xg, up_s, dn_s, act, cs, cr, ys, yr, xs, xb, xr, zb, zr,
+    xg, up_s, dn_s, act, cs, cr, fw, fb, yr, gs, gb, gr, hb, hr, xs, xb, xr, kept, zb, zr,
     s_tz, r_tz, s_tx, r_tx, s_ty, r_ty, s_tc, r_tc,
-    s_up, r_up, s_dn, r_dn, s_c, r_c, s_y, r_y, s_x, r_x, s_z, r_z,
+    s_up, r_up, s_dn, r_dn, s_c, r_c, s_y, r_y, s_g, r_g, s_h, r_h, s_x, r_x, s_z, r_z,
 ):
     f, t = lax.axis_index("fs"), lax.axis_index("tp")
     z, x = f // 2, f % 2
@@ -55,13 +55,15 @@
     low = 1 - z // 2
     far = (3 * low, 1 + low, 1 - z + 4 * (1 - low))
 
+    turn = (far[0] * c + far[2] * (1 - c), far[1], far[2] * c + far[0] * (1 - c))
+
     wide = tok[...].astype(F32)
     scale = lax.rsqrt(jnp.mean(wide * wide, axis=1, keepdims=True) + EPS)
     mine = tok[:, pl.ds(pl.multiple_of(t * cols, cols), cols)].astype(F32)
     xg[t, z, x] = (mine * scale).astype(BF16)
     pl.semaphore_wait(barrier, SUB + 1)
 
-    for zz in far:
+    for zz in turn:
         send(xg.at[t, z, x], xg.at[t, z, x], s_tz.at[zz], r_tz.at[z], (zz * 2 + x, t))
 
     def pass_on(zz):
@@ -82,7 +84,7 @@
         return ref.at[pl.ds(pl.multiple_of(k * feat, feat), feat), :]
 
     def scatter(src, out, ssem, rsem):
-        order = [zz * 2 + xx for zz in far for xx in (x, ox)] + [z * 2 + ox]
+        order = [z * 2 + ox] + [zz * 2 + xx for zz in turn for xx in (x, ox)]
         for dest in order:
             send(src.at[dest], at_rows(out, f), ssem.at[dest], rsem.at[f], (dest, t))
 
@@ -137,6 +139,14 @@
         def _():
             arrived(at_rows(dn_o, k), s_dn.at[k], r_dn.at[k], (k, t))
 
+    def two(h):
+        return pl.ds(h * 2, 2)
+
+    def each(h, body):
+        @pl.loop(0, 2)
+        def _(step):
+            body(h * 2 + step)
+
     def to_core(yy, i):
         k = yy * 4 + oc * 2 + i
         have(k)
@@ -147,49 +157,88 @@
 
         send(cs.at[yy * 2 + i], cr.at[yy * 2 + i], s_c.at[yy, i], r_c.at[yy, i], at_c)
 
-    def core_sum(yy, i):
-        have(yy * 4 + c * 2 + i)
-        arrived(cr.at[yy * 2 + i], s_c.at[yy, i], r_c.at[yy, i], at_c)
-
-    for i in range(2):
-        to_core(oy, i)
-    for i in range(2):
-        core_sum(oy, i)
-
-        @pl.loop(0, nz)
-        def _(zz):
-            ys[i, zz] = (partial(oy * 4 + c * 2 + i, zz) + cr[oy * 2 + i, zz].astype(F32)).astype(BF16)
-
-        send(ys.at[i], yr.at[i], s_y.at[i], r_y.at[i], at_y)
-    for i in range(2):
-        to_core(y, i)
-    for i in range(2):
-        core_sum(y, i)
-        arrived(yr.at[i], s_y.at[i], r_y.at[i], at_y)
-
-        @pl.loop(0, nz)
-        def _(zz):
-            total = (partial(y * 4 + c * 2 + i, zz) + cr[y * 2 + i, zz].astype(F32)
-                     + yr[i, zz].astype(F32))
-            for xx in range(2):
-                half = total[xx * rows:(xx + 1) * rows]
-                xs[i, xx, zz] = half
-                xb[i, xx, zz] = half.astype(BF16)
-
-        send(xb.at[i, ox], xr.at[i], s_x.at[i], r_x.at[i], at_x)
-    for i in range(2):
-        arrived(xr.at[i], s_x.at[i], r_x.at[i], at_x)
-
-        @pl.loop(0, nz)
-        def _(zz):
-            total = xs[i, x, zz] + xr[i, zz].astype(F32)
-            xs[i, x, zz] = total
-            zb[i, zz] = total.astype(BF16)
-
-        for zz in far:
+    def core_sum(yy, i, zz):
+        return partial(yy * 4 + c * 2 + i, zz) + cr[yy * 2 + i, zz].astype(F32)
+
+    def halves(total, wide_ref, sent_ref, zz):
+        for xx in range(2):
+            half = total[xx * rows:(xx + 1) * rows]
+            wide_ref[xx, zz] = half
+            sent_ref[xx, zz] = half.astype(BF16)
+
+    hs = (low, 1 - low)
+    close = z // 2
+    over_y = [
+        pltpu.make_async_remote_copy(
+            src_ref=fb.at[oy, two(h)], dst_ref=yr.at[two(h)], send_sem=s_y.at[h],
+            recv_sem=r_y.at[h], device_id=at_y, device_id_type=pl.DeviceIdType.MESH)
+        for h in hs]
+    sent.extend(over_y)
+
+    for yy in (close, 1 - close):
+        for i in (1, 0):
+            to_core(yy, i)
+        for i in (1, 0):
+            have(yy * 4 + c * 2 + i)
+            arrived(cr.at[yy * 2 + i], s_c.at[yy, i], r_c.at[yy, i], at_c)
+            for h in hs:
+                if i == 1:
+                    each(h, lambda zz: halves(core_sum(yy, 1, zz), gs.at[yy], gb.at[yy], zz))
+                    send(gb.at[yy, ox, two(h)], gr.at[yy, two(h)],
+                         s_g.at[yy, h], r_g.at[yy, h], at_x)
+                else:
+                    def body(zz):
+                        total = core_sum(yy, 0, zz)
+                        fw[yy, zz] = total
+                        fb[yy, zz] = total.astype(BF16)
+
+                    each(h, body)
+
+        @pl.when(yy == oy)
+        def _():
+            for copy in over_y:
+                copy.start()
+
+    for h in hs:
+        arrived(gr.at[oy, two(h)], s_g.at[oy, h], r_g.at[oy, h], at_x)
+
+        def body(zz):
+            hb[zz] = (gs[oy, x, zz] + gr[oy, zz].astype(F32)).astype(BF16)
+
+        each(h, body)
+        send(hb.at[two(h)], hr.at[two(h)], s_h.at[h], r_h.at[h], at_y)
+    for h in hs:
+        arrived(yr.at[two(h)], s_y.at[h], r_y.at[h], at_y)
+        each(h, lambda zz: halves(fw[y, zz] + yr[zz].astype(F32), xs, xb, zz))
+        send(xb.at[ox, two(h)], xr.at[two(h)], s_x.at[h], r_x.at[h], at_x)
+
+    def over_z(i, place):
+        for zz in (far[:2], far[2:])[place]:
             send(zb.at[i, zz], zr.at[i, z], s_z.at[i, zz], r_z.at[i, z], (zz * 2 + x, t))
-    for i in range(2):
-        total = xs[i, x, z]
+
+    for place, h in enumerate(hs):
+        arrived(gr.at[y, two(h)], s_g.at[y, h], r_g.at[y, h], at_x)
+        arrived(hr.at[two(h)], s_h.at[h], r_h.at[h], at_y)
+
+        def body(zz):
+            total = gs[y, x, zz] + gr[y, zz].astype(F32) + hr[zz].astype(F32)
+            kept[1, zz] = total
+            zb[1, zz] = total.astype(BF16)
+
+        each(h, body)
+        over_z(1, place)
+    for place, h in enumerate(hs):
+        arrived(xr.at[two(h)], s_x.at[h], r_x.at[h], at_x)
+
+        def body(zz):
+            total = xs[x, zz] + xr[zz].astype(F32)
+            kept[0, zz] = total
+            zb[0, zz] = total.astype(BF16)
+
+        each(h, body)
+        over_z(0, place)
+    for i in (1, 0):
+        total = kept[i, z]
         for zz in near:
             arrived(zr.at[i, zz], s_z.at[i, zz], r_z.at[i, zz], (zz * 2 + x, t))
             total += zr[i, zz].astype(F32)
@@ -207,7 +256,7 @@
     span = 2 * rows
     dma = pltpu.SemaphoreType.DMA
     vmem = pl.BlockSpec(memory_space=pltpu.VMEM)
-    shapes = [(nz,), (nz,), (nz, 2), (2, 2), (SUB,), (SUB,), (2, 2), (2,), (2,), (2, nz)]
+    shapes = [(nz,), (nz,), (nz, 2), (2, 2), (SUB,), (SUB,), (2, 2), (2,), (2, 2), (2,), (2,), (2, nz)]
     up_s, dn_s, mixed = pl.pallas_call(
         functools.partial(fused, nz),
         out_shape=(
@@ -224,11 +273,18 @@
             pltpu.VMEM((SUB * rows, units), BF16),
             pltpu.VMEM((4, nz, span, feat), BF16),
             pltpu.VMEM((4, nz, span, feat), BF16),
+            pltpu.VMEM((2, nz, span, feat), F32),
             pltpu.VMEM((2, nz, span, feat), BF16),
-            pltpu.VMEM((2, nz, span, feat), BF16),
+            pltpu.VMEM((nz, span, feat), BF16),
             pltpu.VMEM((2, 2, nz, rows, feat), F32),
             pltpu.VMEM((2, 2, nz, rows, feat), BF16),
             pltpu.VMEM((2, nz, rows, feat), BF16),
+            pltpu.VMEM((nz, rows, feat), BF16),
+            pltpu.VMEM((nz, rows, feat), BF16),
+            pltpu.VMEM((2, nz, rows, feat), F32),
+            pltpu.VMEM((2, nz, rows, feat), BF16),
+            pltpu.VMEM((nz, rows, feat), BF16),
+            pltpu.VMEM((2, nz, rows, feat), F32),
             pltpu.VMEM((2, nz, rows, feat), BF16),
             pltpu.VMEM((2, nz, rows, feat), BF16),
         ] + [dma(shape) for shape in shapes for _ in range(2)],

time: 116 us -> 105 us (0.905)
  Pallas kernels: 109 us -> 98.2 us
    pallas_call x1, Pallas kernels: 109 us -> 98.2 us  [on_device_fused(): pl.pallas_call(functools.partial(fused, nz), out_shape=(jax.ShapeDtypeStr...]
where the time goes in v2:
time: 105 us; the launch traced here: 104 us
  Pallas kernels  98.2 us (94%)
  local copies, waits for them, and re-layouts  5.46 us (5%)
    pallas_call x1, Pallas kernels, on_device_fused(): pl.pallas_call(functools.partial(fused, nz), out_shape=(jax.ShapeDtypeStr...  98.2 us
    unnamed x7, local copies, waits for them, and re-layouts  3.99 us

profile of v2, /device:TPU:0, one launch (start us, length us, event | category | flops | bytes accessed | tf_op | source)
XLA Modules:
  0.0 104.3 jit_solution(9106780945168075671)
XLA Ops:
  0.6 1.5 %copy.7.gain = f32[256,1]{1,0:T(8,128)} copy(f32[256,1]{0,1:T(1,128)} %bitcast.5) | data formatting | bytes 2048 | tf_op jit(solution)/shard_map/broadcast_in_dim | solution.py:293
  2.1 98.2 %shard_map.67 = (bf16[2048,256]{1,0:T(8,128)(2,1)}, bf16[2048,256]{1,0:T(8,128)(2,1)}, bf16[128,512]{1,0:T(8,128)(2,1)}) custom-call(bf16[128,2048]{1,0:T(8,128)(2,1)} %tok.1, f32[256,1]{1,0:T(8,128)} %copy.7.gain, f32[256,2048]{1,0:T(8,128)} %upm.1, f32[256,2048]{1,0:T(8,128)} %dnm.1), custom_call_target="tpu_custom_call" | custom-call | tf_op jit(solution)/shard_map/pallas_call | solution.py:260
  100.3 0.0 copy-start
  100.3 0.0 copy-start.1
  100.4 2.4 %copy.11 = bf16[1,2048,256]{2,1,0:T(8,128)(2,1)} copy(bf16[1,2048,256]{2,1,0:T(8,128)(2,1)} %bitcast.4) | data formatting | bytes 2097152
  102.7 0.0 copy-done
  102.7 1.0 copy.12
  103.7 0.0 copy-done.1
  103.7 0.7 copy.13
Async XLA Ops:
  100.3 2.4 %copy-start = (bf16[2048,256]{1,0:T(8,128)(2,1)S(1)}, bf16[2048,256]{1,0:T(8,128)(2,1)}, u32[]{:S(2)}) copy-start(bf16[2048,256]{1,0:T(8,128)(2,1)} %get-tuple-element.7) | copy-start | bytes 3145732
  100.3 3.3 %copy-start.1 = (bf16[128,512]{1,0:T(8,128)(2,1)S(1)}, bf16[128,512]{1,0:T(8,128)(2,1)}, u32[]{:S(2)}) copy-start(bf16[128,512]{1,0:T(8,128)(2,1)} %get-tuple-element.14) | copy-start | bytes 393220

commit v3 on v2

--- a/solution.py
+++ b/solution.py
@@ -14,8 +14,8 @@
 
 
 def fused(
-    nz, tok, gain, upm, dnm, up_o, dn_o, mix_o,
-    xg, up_s, dn_s, act, cs, cr, fw, fb, yr, gs, gb, gr, hb, hr, xs, xb, xr, kept, zb, zr,
+    nz, tok_h, gain, upm_h, dnm_h, up_h, dn_h, mix_o,
+    tok, upm, dnm, up_o, dn_o, s_in, s_out, xg, up_s, dn_s, act, cs, cr, fw, fb, yr, gs, gb, gr, hb, hr, xs, xb, xr, kept, zb, zr,
     s_tz, r_tz, s_tx, r_tx, s_ty, r_ty, s_tc, r_tc,
     s_up, r_up, s_dn, r_dn, s_c, r_c, s_y, r_y, s_g, r_g, s_h, r_h, s_x, r_x, s_z, r_z,
 ):
@@ -31,6 +31,11 @@
     at_y = (f, oy * 2 + c)
     at_c = (f, y * 2 + oc)
 
+    fetch = [pltpu.make_async_copy(src, dst, s_in.at[n]) for n, (src, dst) in enumerate(
+        ((tok_h, tok), (upm_h, upm), (dnm_h, dnm)))]
+    for copy in fetch:
+        copy.start()
+
     barrier = pltpu.get_barrier_semaphore()
     for d in range(1, SUB):
         pl.semaphore_signal(barrier, inc=1, device_id=((f + d) % SUB, t),
@@ -57,6 +62,7 @@
 
     turn = (far[0] * c + far[2] * (1 - c), far[1], far[2] * c + far[0] * (1 - c))
 
+    fetch[0].wait()
     wide = tok[...].astype(F32)
     scale = lax.rsqrt(jnp.mean(wide * wide, axis=1, keepdims=True) + EPS)
     mine = tok[:, pl.ds(pl.multiple_of(t * cols, cols), cols)].astype(F32)
@@ -83,15 +89,20 @@
     def at_rows(ref, k):
         return ref.at[pl.ds(pl.multiple_of(k * feat, feat), feat), :]
 
-    def scatter(src, out, ssem, rsem):
-        order = [z * 2 + ox] + [zz * 2 + xx for zz in turn for xx in (x, ox)]
-        for dest in order:
-            send(src.at[dest], at_rows(out, f), ssem.at[dest], rsem.at[f], (dest, t))
-
-    cast(upm, up_s, up_o, gain[...])
-    scatter(up_s, up_o, s_up, r_up)
+    def order(planes):
+        return [z * 2 + ox] + [zz * 2 + xx for zz in planes for xx in (x, ox)]
+
+    fine = feat // 2
+
+    def at_half(ref, k, i):
+        return ref.at[pl.ds(pl.multiple_of(k * feat + i * fine, fine), fine), :]
+
+    fetch[1].wait()
+    cast(upm, up_s, up_o, jnp.transpose(gain[...]))
+    for dest in order(turn):
+        send(up_s.at[dest], at_rows(up_o, f), s_up.at[dest], r_up.at[f], (dest, t))
+    fetch[2].wait()
     cast(dnm, dn_s, dn_o, None)
-    scatter(dn_s, dn_o, s_dn, r_dn)
 
     near = (far[2], far[1], far[0])
     for zz in near:
@@ -108,6 +119,13 @@
         for zz in (z,) + near:
             arrived(xg.at[other, zz, xx], s_ty.at[zz, xx], r_ty.at[zz, xx], at_y)
         send(xg.at[other, :, xx], xg.at[other, :, xx], s_tc.at[oy, xx], r_tc.at[oy, xx], at_c)
+    def send_down(i, dest):
+        send(dn_s.at[dest, i * fine:(i + 1) * fine], at_half(dn_o, f, i),
+             s_dn.at[i, dest], r_dn.at[i, f], (dest, t))
+
+    for i in range(2):
+        for dest in order(far[2:]):
+            send_down(i, dest)
     for yy in (y, oy):
         for xx in (x, ox):
             part = xg.at[yy * 2 + oc, :, xx]
@@ -116,6 +134,13 @@
     everyone = [zz * 2 + xx for zz in far for xx in (x, ox)] + [z * 2 + ox]
     for k in everyone:
         arrived(at_rows(up_o, k), s_up.at[k], r_up.at[k], (k, t))
+    crossing = (far[0] * c + far[1] * (1 - c), far[1] * c + far[0] * (1 - c))
+    for i in range(2):
+        for zz in crossing:
+            for xx in (x, ox):
+                send_down(i, zz * 2 + xx)
+    keep_up = pltpu.make_async_copy(up_o, up_h, s_out.at[0])
+    keep_up.start()
 
     span = 2 * rows
 
@@ -128,16 +153,21 @@
         act[pl.ds(pl.multiple_of(zz * span, span), span), :] = jnp.square(
             jnp.maximum(total, 0.0)).astype(BF16)
 
-    def partial(k, zz):
-        return lax.dot_general(
-            act[pl.ds(pl.multiple_of(zz * span, span), span), :],
-            dn_o[pl.ds(pl.multiple_of(k * feat, feat), feat), :],
-            (((1,), (1,)), ((), ())), preferred_element_type=F32)
-
-    def have(k):
-        @pl.when(k != f)
-        def _():
-            arrived(at_rows(dn_o, k), s_dn.at[k], r_dn.at[k], (k, t))
+    def partial(yy, cc, i, zz):
+        rows_act = act[pl.ds(pl.multiple_of(zz * span, span), span), :]
+        return jnp.concatenate([
+            lax.dot_general(
+                rows_act, at_half(dn_o, yy * 4 + cc * 2 + xx, i)[...],
+                (((1,), (1,)), ((), ())), preferred_element_type=F32)
+            for xx in range(2)], axis=1)
+
+    def have(yy, cc, i):
+        for xx in range(2):
+            k = yy * 4 + cc * 2 + xx
+
+            @pl.when(k != f)
+            def _():
+                arrived(at_half(dn_o, k, i), s_dn.at[i, k], r_dn.at[i, k], (k, t))
 
     def two(h):
         return pl.ds(h * 2, 2)
@@ -148,17 +178,16 @@
             body(h * 2 + step)
 
     def to_core(yy, i):
-        k = yy * 4 + oc * 2 + i
-        have(k)
+        have(yy, oc, i)
 
         @pl.loop(0, nz)
         def _(zz):
-            cs[yy * 2 + i, zz] = partial(k, zz).astype(BF16)
+            cs[yy * 2 + i, zz] = partial(yy, oc, i, zz).astype(BF16)
 
         send(cs.at[yy * 2 + i], cr.at[yy * 2 + i], s_c.at[yy, i], r_c.at[yy, i], at_c)
 
     def core_sum(yy, i, zz):
-        return partial(yy * 4 + c * 2 + i, zz) + cr[yy * 2 + i, zz].astype(F32)
+        return partial(yy, c, i, zz) + cr[yy * 2 + i, zz].astype(F32)
 
     def halves(total, wide_ref, sent_ref, zz):
         for xx in range(2):
@@ -175,47 +204,75 @@
         for h in hs]
     sent.extend(over_y)
 
-    for yy in (close, 1 - close):
-        for i in (1, 0):
-            to_core(yy, i)
-        for i in (1, 0):
-            have(yy * 4 + c * 2 + i)
-            arrived(cr.at[yy * 2 + i], s_c.at[yy, i], r_c.at[yy, i], at_c)
-            for h in hs:
-                if i == 1:
-                    each(h, lambda zz: halves(core_sum(yy, 1, zz), gs.at[yy], gb.at[yy], zz))
-                    send(gb.at[yy, ox, two(h)], gr.at[yy, two(h)],
-                         s_g.at[yy, h], r_g.at[yy, h], at_x)
-                else:
-                    def body(zz):
-                        total = core_sum(yy, 0, zz)
-                        fw[yy, zz] = total
-                        fb[yy, zz] = total.astype(BF16)
-
-                    each(h, body)
-
-        @pl.when(yy == oy)
-        def _():
-            for copy in over_y:
-                copy.start()
-
-    for h in hs:
-        arrived(gr.at[oy, two(h)], s_g.at[oy, h], r_g.at[oy, h], at_x)
-
-        def body(zz):
-            hb[zz] = (gs[oy, x, zz] + gr[oy, zz].astype(F32)).astype(BF16)
-
-        each(h, body)
-        send(hb.at[two(h)], hr.at[two(h)], s_h.at[h], r_h.at[h], at_y)
+    def stage(i, yy):
+        to_core(yy, i)
+        have(yy, c, i)
+        arrived(cr.at[yy * 2 + i], s_c.at[yy, i], r_c.at[yy, i], at_c)
+        for h in hs:
+            if i == 1:
+                each(h, lambda zz: halves(core_sum(yy, 1, zz), gs.at[yy], gb.at[yy], zz))
+                send(gb.at[yy, ox, two(h)], gr.at[yy, two(h)],
+                     s_g.at[yy, h], r_g.at[yy, h], at_x)
+            else:
+                def body(zz):
+                    total = core_sum(yy, 0, zz)
+                    fw[yy, zz] = total
+                    fb[yy, zz] = total.astype(BF16)
+
+                each(h, body)
+        if i == 0:
+            @pl.when(yy == oy)
+            def _():
+                for copy in over_y:
+                    copy.start()
+
+    pair, same = far[2], (z + 2) % 4
+    across = (pair + 2) % 4
+    at_pair, at_same = (pair * 2 + x, t), (same * 2 + x, t)
+
+    def to_pair(i, place):
+        if place == 0:
+            send(zb.at[i, across], zr.at[i, 0], s_z.at[i, 0], r_z.at[i, 0], at_pair)
+        else:
+            send(zb.at[i, pair], zr.at[i, 1], s_z.at[i, 1], r_z.at[i, 1], at_pair)
+
+    def cross(i):
+        arrived(zr.at[i, 0], s_z.at[i, 0], r_z.at[i, 0], at_pair)
+        zb[i, z] = (kept[i, same] + zr[i, 0].astype(F32)).astype(BF16)
+        send(zb.at[i, z], zr.at[i, 2], s_z.at[i, 2], r_z.at[i, 2], at_same)
+
+    stage(0, close)
+    stage(1, close)
+    stage(0, 1 - close)
     for h in hs:
         arrived(yr.at[two(h)], s_y.at[h], r_y.at[h], at_y)
         each(h, lambda zz: halves(fw[y, zz] + yr[zz].astype(F32), xs, xb, zz))
         send(xb.at[ox, two(h)], xr.at[two(h)], s_x.at[h], r_x.at[h], at_x)
-
-    def over_z(i, place):
-        for zz in (far[:2], far[2:])[place]:
-            send(zb.at[i, zz], zr.at[i, z], s_z.at[i, zz], r_z.at[i, z], (zz * 2 + x, t))
-
+    stage(1, 1 - close)
+    keep_dn = pltpu.make_async_copy(dn_o, dn_h, s_out.at[1])
+    keep_dn.start()
+    for place, h in enumerate(hs):
+        arrived(gr.at[oy, two(h)], s_g.at[oy, h], r_g.at[oy, h], at_x)
+
+        def body(zz):
+            hb[zz] = (gs[oy, x, zz] + gr[oy, zz].astype(F32)).astype(BF16)
+
+        each(h, body)
+        send(hb.at[two(h)], hr.at[two(h)], s_h.at[h], r_h.at[h], at_y)
+    for place, h in enumerate(hs):
+        arrived(xr.at[two(h)], s_x.at[h], r_x.at[h], at_x)
+
+        def body(zz):
+            total = xs[x, zz] + xr[zz].astype(F32)
+            kept[0, zz] = total
+
+            @pl.when(zz != z)
+            def _():
+                zb[0, zz] = total.astype(BF16)
+
+        each(h, body)
+        to_pair(0, place)
+    cross(0)
     for place, h in enumerate(hs):
         arrived(gr.at[y, two(h)], s_g.at[y, h], r_g.at[y, h], at_x)
         arrived(hr.at[two(h)], s_h.at[h], r_h.at[h], at_y)
@@ -223,28 +280,26 @@
         def body(zz):
             total = gs[y, x, zz] + gr[y, zz].astype(F32) + hr[zz].astype(F32)
             kept[1, zz] = total
-            zb[1, zz] = total.astype(BF16)
+
+            @pl.when(zz != z)
+            def _():
+                zb[1, zz] = total.astype(BF16)
 
         each(h, body)
-        over_z(1, place)
-    for place, h in enumerate(hs):
-        arrived(xr.at[two(h)], s_x.at[h], r_x.at[h], at_x)
-
-        def body(zz):
-            total = xs[x, zz] + xr[zz].astype(F32)
-            kept[0, zz] = total
-            zb[0, zz] = total.astype(BF16)
-
-        each(h, body)
-        over_z(0, place)
-    for i in (1, 0):
-        total = kept[i, z]
-        for zz in near:
-            arrived(zr.at[i, zz], s_z.at[i, zz], r_z.at[i, zz], (zz * 2 + x, t))
-            total += zr[i, zz].astype(F32)
-        mix_o[:, i * feat:(i + 1) * feat] = total.astype(BF16)
+        to_pair(1, place)
+        if place == 0:
+            cross(1)
+    for i in range(2):
+        arrived(zr.at[i, 1], s_z.at[i, 1], r_z.at[i, 1], at_pair)
+        arrived(zr.at[i, 2], s_z.at[i, 2], r_z.at[i, 2], at_same)
+        total = (kept[i, z] + zr[i, 1].astype(F32) + zr[i, 2].astype(F32)).astype(BF16)
+        for xx in range(2):
+            mix_o[:, xx * feat + i * fine:xx * feat + (i + 1) * fine] = (
+                total[:, xx * fine:(xx + 1) * fine])
     for copy in sent:
         copy.wait_send()
+    keep_up.wait()
+    keep_dn.wait()
 
 
 def on_device_fused(tokens, gain, up_master, down_master):
@@ -256,7 +311,8 @@
     span = 2 * rows
     dma = pltpu.SemaphoreType.DMA
     vmem = pl.BlockSpec(memory_space=pltpu.VMEM)
-    shapes = [(nz,), (nz,), (nz, 2), (2, 2), (SUB,), (SUB,), (2, 2), (2,), (2, 2), (2,), (2,), (2, nz)]
+    anywhere = pl.BlockSpec(memory_space=pl.ANY)
+    shapes = [(nz,), (nz,), (nz, 2), (2, 2), (SUB,), (2, SUB), (2, 2), (2,), (2, 2), (2,), (2,), (2, nz)]
     up_s, dn_s, mixed = pl.pallas_call(
         functools.partial(fused, nz),
         out_shape=(
@@ -264,9 +320,16 @@
             jax.ShapeDtypeStruct((SUB * feat, units), BF16),
             jax.ShapeDtypeStruct((rows, cols), BF16),
         ),
-        in_specs=[vmem] * 4,
-        out_specs=(vmem,) * 3,
+        in_specs=[anywhere, vmem, anywhere, anywhere],
+        out_specs=(anywhere, anywhere, vmem),
         scratch_shapes=[
+            pltpu.VMEM((rows, width), BF16),
+            pltpu.VMEM((feat, ff), F32),
+            pltpu.VMEM((feat, ff), F32),
+            pltpu.VMEM((SUB * feat, units), BF16),
+            pltpu.VMEM((SUB * feat, units), BF16),
+            dma((3,)),
+            dma((2,)),
             pltpu.VMEM((4, nz, 2, rows, cols), BF16),
             pltpu.VMEM((SUB, feat, units), BF16),
             pltpu.VMEM((SUB, feat, units), BF16),
@@ -290,7 +353,7 @@
         ] + [dma(shape) for shape in shapes for _ in range(2)],
         compiler_params=pltpu.CompilerParams(
             collective_id=0, has_side_effects=True, vmem_limit_bytes=60 * 2**20),
-    )(tokens, gain[:, None], up_master, down_master)
+    )(tokens, gain[None, :], up_master, down_master)
     return up_s[None], dn_s[None], mixed
 
 

time: 105 us -> 97.8 us (0.931)
  Pallas kernels: 98.2 us -> 93 us
  local copies, waits for them, and re-layouts: 5.46 us -> 3.99 us
    pallas_call x1, Pallas kernels: 98.2 us -> 93 us  [on_device_fused(): pl.pallas_call(functools.partial(fused, nz), out_shape=(jax.ShapeDtypeStr...]
    broadcast_in_dim x1 -> x0, local copies, waits for them, and re-layouts: 1.47 us -> none  [on_device_fused(): gain[:, None]]
where the time goes in v3:
time: 97.8 us; the launch traced here: 97.6 us
  Pallas kernels  93 us (95%)
  local copies, waits for them, and re-layouts  3.99 us (4%)
    pallas_call x1, Pallas kernels, on_device_fused(): pl.pallas_call(functools.partial(fused, nz), out_shape=(jax.ShapeDtypeStr...  93 us
    unnamed x7, local copies, waits for them, and re-layouts  3.99 us

profile of v3, /device:TPU:0, one launch (start us, length us, event | category | flops | bytes accessed | tf_op | source)
XLA Modules:
  0.0 97.6 jit_solution(16374392255669133620)
XLA Ops:
  0.6 93.0 %shard_map.67 = (bf16[2048,256]{1,0:T(8,128)(2,1)}, bf16[2048,256]{1,0:T(8,128)(2,1)}, bf16[128,512]{1,0:T(8,128)(2,1)}) custom-call(bf16[128,2048]{1,0:T(8,128)(2,1)} %tok_h.1, f32[1,256]{1,0:T(1,128)} %bitcast.5, f32[256,2048]{1,0:T(8,128)} %upm_h.1, f32[256,2048]{1,0:T(8,128)} %dnm_h.1), custom_call_target="tpu_custom_call" | custom-call | tf_op jit(solution)/shard_map/pallas_call | solution.py:316
  93.6 0.0 copy-start
  93.6 0.0 copy-start.1
  93.6 2.4 %copy.10 = bf16[1,2048,256]{2,1,0:T(8,128)(2,1)} copy(bf16[1,2048,256]{2,1,0:T(8,128)(2,1)} %bitcast.4) | data formatting | bytes 2097152
  96.0 0.0 copy-done
  96.0 1.0 copy.11
  97.0 0.0 copy-done.1
  97.0 0.7 copy.12
Async XLA Ops:
  93.6 2.4 %copy-start = (bf16[2048,256]{1,0:T(8,128)(2,1)S(1)}, bf16[2048,256]{1,0:T(8,128)(2,1)}, u32[]{:S(2)}) copy-start(bf16[2048,256]{1,0:T(8,128)(2,1)} %get-tuple-element.7) | copy-start | bytes 3145732
  93.6 3.3 %copy-start.1 = (bf16[128,512]{1,0:T(8,128)(2,1)S(1)}, bf16[128,512]{1,0:T(8,128)(2,1)}, u32[]{:S(2)}) copy-start(bf16[128,512]{1,0:T(8,128)(2,1)} %get-tuple-element.14) | copy-start | bytes 393220

commit v4 on v3

--- a/solution.py
+++ b/solution.py
@@ -241,24 +241,35 @@
         zb[i, z] = (kept[i, same] + zr[i, 0].astype(F32)).astype(BF16)
         send(zb.at[i, z], zr.at[i, 2], s_z.at[i, 2], r_z.at[i, 2], at_same)
 
+    over_h = [
+        pltpu.make_async_remote_copy(
+            src_ref=hb.at[two(h)], dst_ref=hr.at[two(h)], send_sem=s_h.at[h],
+            recv_sem=r_h.at[h], device_id=at_y, device_id_type=pl.DeviceIdType.MESH)
+        for h in hs]
+    sent.extend(over_h)
+
+    def other_half():
+        for place, h in enumerate(hs):
+            arrived(gr.at[oy, two(h)], s_g.at[oy, h], r_g.at[oy, h], at_x)
+
+            def body(zz):
+                hb[zz] = (gs[oy, x, zz] + gr[oy, zz].astype(F32)).astype(BF16)
+
+            each(h, body)
+            over_h[place].start()
+
     stage(0, close)
     stage(1, close)
     stage(0, 1 - close)
+    pl.when(oy == close)(other_half)
+    stage(1, 1 - close)
     for h in hs:
         arrived(yr.at[two(h)], s_y.at[h], r_y.at[h], at_y)
         each(h, lambda zz: halves(fw[y, zz] + yr[zz].astype(F32), xs, xb, zz))
         send(xb.at[ox, two(h)], xr.at[two(h)], s_x.at[h], r_x.at[h], at_x)
-    stage(1, 1 - close)
+    pl.when(oy != close)(other_half)
     keep_dn = pltpu.make_async_copy(dn_o, dn_h, s_out.at[1])
     keep_dn.start()
-    for place, h in enumerate(hs):
-        arrived(gr.at[oy, two(h)], s_g.at[oy, h], r_g.at[oy, h], at_x)
-
-        def body(zz):
-            hb[zz] = (gs[oy, x, zz] + gr[oy, zz].astype(F32)).astype(BF16)
-
-        each(h, body)
-        send(hb.at[two(h)], hr.at[two(h)], s_h.at[h], r_h.at[h], at_y)
     for place, h in enumerate(hs):
         arrived(xr.at[two(h)], s_x.at[h], r_x.at[h], at_x)
 

time: 97.8 us -> 96.9 us (level)
  no operation moved by 1% of the time
where the time goes in v4:
time: 96.9 us; the launch traced here: 96.7 us
  Pallas kernels  92.1 us (95%)
  local copies, waits for them, and re-layouts  3.99 us (4%)
    pallas_call x1, Pallas kernels, on_device_fused(): pl.pallas_call(functools.partial(fused, nz), out_shape=(jax.ShapeDtypeStr...  92.1 us
    unnamed x7, local copies, waits for them, and re-layouts  3.99 us

profile of v4, /device:TPU:0, one launch (start us, length us, event | category | flops | bytes accessed | tf_op | source)
XLA Modules:
  0.0 96.7 jit_solution(12488166744574095489)
XLA Ops:
  0.6 92.1 %shard_map.67 = (bf16[2048,256]{1,0:T(8,128)(2,1)}, bf16[2048,256]{1,0:T(8,128)(2,1)}, bf16[128,512]{1,0:T(8,128)(2,1)}) custom-call(bf16[128,2048]{1,0:T(8,128)(2,1)} %tok_h.1, f32[1,256]{1,0:T(1,128)} %bitcast.5, f32[256,2048]{1,0:T(8,128)} %upm_h.1, f32[256,2048]{1,0:T(8,128)} %dnm_h.1), custom_call_target="tpu_custom_call" | custom-call | tf_op jit(solution)/shard_map/pallas_call | solution.py:327
  92.7 0.0 copy-start
  92.7 0.0 copy-start.1
  92.7 2.4 %copy.10 = bf16[1,2048,256]{2,1,0:T(8,128)(2,1)} copy(bf16[1,2048,256]{2,1,0:T(8,128)(2,1)} %bitcast.4) | data formatting | bytes 2097152
  95.1 0.0 copy-done
  95.1 1.0 %copy.11 = bf16[1,2048,256]{2,1,0:T(8,128)(2,1)} copy(bf16[1,2048,256]{2,1,0:T(8,128)(2,1)S(1)} %bitcast.3) | data formatting | bytes 2097152
  96.1 0.0 copy-done.1
  96.1 0.7 copy.12
Async XLA Ops:
  92.7 2.4 %copy-start = (bf16[2048,256]{1,0:T(8,128)(2,1)S(1)}, bf16[2048,256]{1,0:T(8,128)(2,1)}, u32[]{:S(2)}) copy-start(bf16[2048,256]{1,0:T(8,128)(2,1)} %get-tuple-element.7) | copy-start | bytes 3145732
  92.7 3.3 %copy-start.1 = (bf16[128,512]{1,0:T(8,128)(2,1)S(1)}, bf16[128,512]{1,0:T(8,128)(2,1)}, u32[]{:S(2)}) copy-start(bf16[128,512]{1,0:T(8,128)(2,1)} %get-tuple-element.14) | copy-start | bytes 393220
